TPU v7x, 32 devices: a whole 2x2x4 slice. The times are simulated.
32 devices in a mesh: sp: 8 (over z, y), dp: 4 (over x, core).
Axes of the slice: x: 2, y: 2, z: 4, core: 2. Of those that a mesh axis runs over, the one named last changes fastest.
Arguments:
- stream: bfloat16 [4, 1024, 2048], P('dp', 'sp'), may hold values from -6 to 6
- queries: bfloat16 [4, 1024, 1024], P('dp', 'sp'), may hold values from -6 to 6
- keys_in: bfloat16 [4, 1024, 1024], P('dp', 'sp'), may hold values from -6 to 6
- values_in: bfloat16 [4, 1024, 1024], P('dp', 'sp'), may hold values from -6 to 6
- key_shift: bfloat16 [4, 1024, 16], P('dp', 'sp'), may hold values from -8 to 16
- head_shift: float32 [16], replicated, may hold values from -16 to 0
- mix_gain: float32 [1024], replicated, may hold values from 0.1 to 1.9
- out_weight: bfloat16 [1024, 2048], replicated, may hold values from -0.1875 to 0.1875
- post_gain: float32 [2048], replicated, may hold values from 0.1 to 1.9
- route: int32 [4, 1024, 2], P('dp', 'sp'), may hold values from 0 to 31, as said below
- route_weight: float32 [4, 1024, 2], P('dp', 'sp'), may hold values from 0.25 to 1
- w_gate: bfloat16 [32, 2048, 1024], P(('sp', 'dp')), may hold values from -0.125 to 0.125
- w_up: bfloat16 [32, 2048, 1024], P(('sp', 'dp')), may hold values from -0.125 to 0.125
- w_down: bfloat16 [32, 1024, 2048], P(('sp', 'dp')), may hold values from -0.1875 to 0.1875
Outputs:
- result: bfloat16 [4, 1024, 2048], P('dp', 'sp')
Inputs may be any that keep to these rules, and one draw needn't show every extreme that they name: `route`: each token names two different experts of one group (the group of expert e is e // 8). Of the 128 tokens of one device, each expert is named by at most 16; in every draw the 8 experts of one group are each named by exactly 16 tokens of every device.
All inputs are finite; a program needn't handle non-finite values.
Results may differ from a plain program's by a relative error of at most 0.0085.
Values may be sent and summed in bfloat16 or wider, within the bound.
A program may use at most 128 MiB of HBM per device.

v0:
```python
import functools
import math

import jax
import jax.numpy as jnp
from jax import lax
from jax.experimental import pallas as pl
from jax.experimental.pallas import tpu as pltpu
from jax.sharding import PartitionSpec as P

HD = 64
GROUPS = 4
MESH = pl.DeviceIdType.MESH
F32 = jnp.float32
BF16 = jnp.bfloat16
VLIM = 56 * 1024 * 1024

norm_eps = 1e-05


def vmem(count):
    return [pl.BlockSpec(memory_space=pltpu.VMEM)] * count


def swap_kernel(n, count, *refs):
    ins, outs = refs[:count], refs[count : 2 * count]
    send_sem, recv_sem, own_sem = refs[2 * count :]
    me = lax.axis_index("sp")
    dp = lax.axis_index("dp")
    barrier = pltpu.get_barrier_semaphore()
    for d in range(1, n):
        pl.semaphore_signal(
            barrier, inc=1, device_id=(lax.rem(me + d, n), dp), device_id_type=MESH
        )
    own = [
        pltpu.make_async_copy(ins[a].at[me], outs[a].at[me], own_sem.at[a]) for a in range(count)
    ]
    for copy in own:
        copy.start()
    pl.semaphore_wait(barrier, n - 1)
    copies = []
    for d in range(1, n):
        peer = lax.rem(me + d, n)
        for a in range(count):
            copies.append(
                pltpu.make_async_remote_copy(
                    src_ref=ins[a].at[peer],
                    dst_ref=outs[a].at[me],
                    send_sem=send_sem.at[a, d],
                    recv_sem=recv_sem.at[a, d],
                    device_id=(peer, dp),
                    device_id_type=MESH,
                )
            )
            copies[-1].start()
    for copy in own + copies:
        copy.wait()


def swap(n, collective, *arrays):
    count = len(arrays)
    return pl.pallas_call(
        functools.partial(swap_kernel, n, count),
        out_shape=[jax.ShapeDtypeStruct(a.shape, a.dtype) for a in arrays],
        in_specs=vmem(count),
        out_specs=vmem(count),
        scratch_shapes=[
            pltpu.SemaphoreType.DMA((count, n)),
            pltpu.SemaphoreType.DMA((count, n)),
            pltpu.SemaphoreType.DMA((count,)),
        ],
        compiler_params=pltpu.CompilerParams(
            collective_id=collective, has_side_effects=True, vmem_limit_bytes=VLIM
        ),
        name=f"swap{collective}",
    )(*arrays)


def attention_kernel(heads, qkv_ref, shift_ref, out_ref):
    blocks, rows, _ = qkv_ref.shape
    cols = heads * HD
    scale = 1.0 / math.sqrt(HD)
    row = lax.broadcasted_iota(jnp.int32, (2 * rows, 2 * rows), 0)
    col = lax.broadcasted_iota(jnp.int32, (2 * rows, 2 * rows), 1)
    source = jnp.where(row >= rows, row - rows, row)
    summer = jnp.where((col >= rows) | (source > col), 1.0, 0.0).astype(BF16)
    causal = lax.broadcasted_iota(jnp.int32, (rows, rows), 1) < lax.broadcasted_iota(
        jnp.int32, (rows, rows), 0
    )

    def tile(i, j, h, carry, total, diagonal):
        q = qkv_ref[i, :, h * HD : (h + 1) * HD]
        k = qkv_ref[j, :, cols + h * HD : cols + (h + 1) * HD]
        v = qkv_ref[j, :, 2 * cols + h * HD : 2 * cols + (h + 1) * HD]
        z = lax.dot_general(q, k, (((1,), (1,)), ((), ())), preferred_element_type=F32) * scale
        z = z + shift_ref[j, h : h + 1, :]
        soft = jnp.log(1.0 + jnp.exp(-jnp.abs(z)))
        breaks = -jnp.maximum(z, 0.0) - soft
        own = jnp.minimum(z, 0.0) - soft
        if diagonal:
            breaks = jnp.where(causal, breaks, 0.0)
        high = breaks.astype(BF16)
        low = (breaks - high.astype(F32)).astype(BF16)
        sums = jnp.dot(
            jnp.concatenate([high, low], axis=1), summer, preferred_element_type=F32
        )
        weight = jnp.exp(own + (sums[:, :rows] + carry))
        if diagonal:
            weight = jnp.where(causal, weight, 0.0)
        total = total + jnp.dot(weight.astype(BF16), v, preferred_element_type=F32)
        return carry + sums[:, rows:], total

    zero_carry = jnp.zeros((rows, rows), F32)
    zero_total = jnp.zeros((rows, HD), F32)

    for i in range(blocks):
        state = []
        for h in range(heads):
            state.extend(tile(i, i, h, zero_carry, zero_total, True))
        for j in range(i - 1, -1, -1):
            new = []
            for h in range(heads):
                new.extend(tile(i, j, h, state[2 * h], state[2 * h + 1], False))
            state = new
        out_ref[i] = jnp.concatenate([state[2 * h + 1] for h in range(heads)], axis=1).astype(BF16)


def attention(heads, qkv, shift):
    blocks, rows, _ = qkv.shape
    return pl.pallas_call(
        functools.partial(attention_kernel, heads),
        out_shape=jax.ShapeDtypeStruct((blocks, rows, heads * HD), BF16),
        in_specs=vmem(2),
        out_specs=vmem(1)[0],
        compiler_params=pltpu.CompilerParams(vmem_limit_bytes=VLIM),
        name="attention",
    )(qkv, shift)


def place(n_sp, n_dp):
    ny = n_sp // GROUPS
    sp, dp = lax.axis_index("sp"), lax.axis_index("dp")
    plane, y = sp // ny, lax.rem(sp, ny)
    member = y * n_dp + dp

    def at(g, m):
        return (g * ny + m // n_dp, lax.rem(m, n_dp))

    return plane, member, at


def greet(plane, member, at, per_group):
    barrier = pltpu.get_barrier_semaphore()
    for d in range(1, GROUPS):
        pl.semaphore_signal(
            barrier, inc=1, device_id=at(lax.rem(plane + d, GROUPS), member), device_id_type=MESH
        )
    for d in range(1, per_group):
        pl.semaphore_signal(
            barrier, inc=1, device_id=at(plane, lax.rem(member + d, per_group)), device_id_type=MESH
        )
    pl.semaphore_wait(barrier, GROUPS + per_group - 2)


def one_hot_rows(meta, row):
    lanes = lax.broadcasted_iota(jnp.int32, (meta.shape[1], meta.shape[1]), 0).astype(F32)
    return lanes == meta[row : row + 1, :]


def dispatch_kernel(
    n_sp,
    n_dp,
    packed,
    meta,
    got,
    got_meta,
    block,
    stage,
    z_send,
    z_recv,
    t_send,
    t_recv,
    p_send,
    p_recv,
    own_sem,
):
    _, per_group, cap, width = got.shape
    slots = packed.shape[1]
    chunk = min(512, width)
    plane, member, at = place(n_sp, n_dp)
    greet(plane, member, at, per_group)
    z_copies, t_copies = [None], [None]
    for d in range(1, GROUPS):
        other = lax.rem(plane + d, GROUPS)
        for kept, src, dst, send, recv in (
            (t_copies, meta, got_meta, t_send, t_recv),
            (z_copies, packed, block, z_send, z_recv),
        ):
            kept.append(
                pltpu.make_async_remote_copy(
                    src_ref=src.at[other],
                    dst_ref=dst.at[plane],
                    send_sem=send.at[d],
                    recv_sem=recv.at[d],
                    device_id=at(other, member),
                    device_id_type=MESH,
                )
            )
            kept[-1].start()
    got_meta[plane] = meta[plane]
    later = []
    for d in range(GROUPS):
        source = lax.rem(plane - d + GROUPS, GROUPS)
        if d:
            t_copies[d].wait_recv()
            z_copies[d].wait_recv()
        held = block if d else packed
        info = got_meta[source]
        hot = jnp.where(one_hot_rows(info, 0) | one_hot_rows(info, 1), 1.0, 0.0).astype(BF16)
        hot = hot[:, :slots]
        for c in range(0, width, chunk):
            rows = jnp.dot(hot, held[source, :, c : c + chunk], preferred_element_type=F32)
            for m in range(per_group):
                stage[source, m, :, c : c + chunk] = rows[m * cap : (m + 1) * cap].astype(BF16)
        own = pltpu.make_async_copy(stage.at[source, member], got.at[source, member], own_sem.at[d])
        own.start()
        later.append(own)
        for e in range(1, per_group):
            other = lax.rem(member + e, per_group)
            copy = pltpu.make_async_remote_copy(
                src_ref=stage.at[source, other],
                dst_ref=got.at[source, member],
                send_sem=p_send.at[d, e],
                recv_sem=p_recv.at[d, e],
                device_id=at(plane, other),
                device_id_type=MESH,
            )
            copy.start()
            later.append(copy)
    for copy in later:
        copy.wait()
    for d in range(1, GROUPS):
        t_copies[d].wait_send()
        z_copies[d].wait_send()


def dispatch(n_sp, n_dp, cap, packed, meta):
    per_group = n_sp * n_dp // GROUPS
    _, slots, width = packed.shape
    buffer = (GROUPS, per_group, cap, width)
    dma = pltpu.SemaphoreType.DMA
    return pl.pallas_call(
        functools.partial(dispatch_kernel, n_sp, n_dp),
        out_shape=[
            jax.ShapeDtypeStruct(buffer, BF16),
            jax.ShapeDtypeStruct(meta.shape, F32),
        ],
        in_specs=vmem(2),
        out_specs=vmem(2),
        scratch_shapes=[
            pltpu.VMEM(packed.shape, BF16),
            pltpu.VMEM(buffer, BF16),
            dma((GROUPS,)),
            dma((GROUPS,)),
            dma((GROUPS,)),
            dma((GROUPS,)),
            dma((GROUPS, per_group)),
            dma((GROUPS, per_group)),
            dma((GROUPS,)),
        ],
        compiler_params=pltpu.CompilerParams(
            collective_id=2, has_side_effects=True, vmem_limit_bytes=VLIM
        ),
        name="dispatch",
    )(packed, meta)


def combine_kernel(
    n_sp,
    n_dp,
    reply,
    meta,
    out,
    block,
    stage,
    z_send,
    z_recv,
    p_send,
    p_recv,
    own_sem,
):
    _, per_group, cap, width = reply.shape
    slots = out.shape[1]
    chunk = min(512, width)
    plane, member, at = place(n_sp, n_dp)
    greet(plane, member, at, per_group)
    order = list(range(1, GROUPS)) + [0]
    plane_copies = {}
    for d in order:
        target = lax.rem(plane + d, GROUPS)
        own = pltpu.make_async_copy(reply.at[target, member], block.at[target, member], own_sem.at[d])
        own.start()
        copies = [own]
        for e in range(1, per_group):
            other = lax.rem(member + e, per_group)
            copies.append(
                pltpu.make_async_remote_copy(
                    src_ref=reply.at[target, other],
                    dst_ref=block.at[target, member],
                    send_sem=p_send.at[d, e],
                    recv_sem=p_recv.at[d, e],
                    device_id=at(plane, other),
                    device_id_type=MESH,
                )
            )
            copies[-1].start()
        plane_copies[d] = copies
    z_copies = []
    for d in order:
        target = lax.rem(plane + d, GROUPS)
        for copy in plane_copies[d]:
            copy.wait()
        info = meta[target]
        spread = jnp.where(one_hot_rows(info, 0), info[2:3, :], 0.0) + jnp.where(
            one_hot_rows(info, 1), info[3:4, :], 0.0
        )
        spread = spread.T[:slots]
        high = spread.astype(BF16)
        low = (spread - high.astype(F32)).astype(BF16)
        for c in range(0, width, chunk):
            if cap % 16 == 0:
                rows = block[target, :, :, c : c + chunk].reshape(per_group * cap, chunk)
            else:
                rows = jnp.concatenate(
                    [block[target, m, :, c : c + chunk].astype(F32) for m in range(per_group)], axis=0
                ).astype(BF16)
            total = jnp.dot(high, rows, preferred_element_type=F32) + jnp.dot(
                low, rows, preferred_element_type=F32
            )
            if d:
                stage[target, :, c : c + chunk] = total.astype(BF16)
            else:
                out[target, :, c : c + chunk] = total.astype(BF16)
        if d:
            copy = pltpu.make_async_remote_copy(
                src_ref=stage.at[target],
                dst_ref=out.at[plane],
                send_sem=z_send.at[d],
                recv_sem=z_recv.at[d],
                device_id=at(target, member),
                device_id_type=MESH,
            )
            copy.start()
            z_copies.append(copy)
    for copy in z_copies:
        copy.wait()


def combine(n_sp, n_dp, slots, reply, meta):
    _, per_group, cap, width = reply.shape
    dma = pltpu.SemaphoreType.DMA
    return pl.pallas_call(
        functools.partial(combine_kernel, n_sp, n_dp),
        out_shape=jax.ShapeDtypeStruct((GROUPS, slots, width), BF16),
        in_specs=vmem(2),
        out_specs=vmem(1)[0],
        scratch_shapes=[
            pltpu.VMEM(reply.shape, BF16),
            pltpu.VMEM((GROUPS, slots, width), BF16),
            dma((GROUPS,)),
            dma((GROUPS,)),
            dma((GROUPS, per_group)),
            dma((GROUPS, per_group)),
            dma((GROUPS,)),
        ],
        compiler_params=pltpu.CompilerParams(
            collective_id=3, has_side_effects=True, vmem_limit_bytes=VLIM
        ),
        name="combine",
    )(reply, meta)


def on_device(
    n_sp,
    n_dp,
    stream,
    queries,
    keys_in,
    values_in,
    key_shift,
    head_shift,
    mix_gain,
    out_weight,
    post_gain,
    route,
    route_weight,
    w_gate,
    w_up,
    w_down,
):
    tokens, width = stream.shape[1], stream.shape[2]
    heads = key_shift.shape[2] // n_sp
    cols = heads * HD

    n_expert = n_sp * n_dp
    per_group = n_expert // GROUPS
    cap = tokens // per_group
    slots = tokens // 2
    expert_ids = route[0].reshape(tokens * 2)
    onehot = (expert_ids[:, None] == jnp.arange(n_expert, dtype=jnp.int32)[None, :]).astype(BF16)
    before = jnp.arange(tokens * 2)
    earlier = (before[:, None] > before[None, :]).astype(BF16)
    counts = jnp.dot(earlier, onehot, preferred_element_type=F32)
    ranks = jnp.sum(counts * onehot.astype(F32), axis=1)
    inside = lax.rem(expert_ids, per_group).astype(F32) * cap + ranks
    inside = inside.reshape(tokens, 2)
    token_group = route[0][:, 0] // per_group
    group_hot = (token_group[:, None] == jnp.arange(GROUPS, dtype=jnp.int32)[None, :]).astype(BF16)
    group_rank = jnp.sum(
        jnp.dot(earlier[:tokens, :tokens], group_hot, preferred_element_type=F32)
        * group_hot.astype(F32),
        axis=1,
    )
    slot = token_group * slots + group_rank.astype(jnp.int32)
    slot_hot = slot[None, :] == jnp.arange(GROUPS * slots, dtype=jnp.int32)[:, None]
    facts = jnp.concatenate([inside + 1.0, route_weight[0]], axis=1)
    table = jnp.sum(jnp.where(slot_hot[:, None, :], facts.T[None, :, :], 0.0), axis=2)
    table = table - jnp.array([1.0, 1.0, 0.0, 0.0], F32)[None, :]
    table = table.reshape(GROUPS, slots, 4).transpose(0, 2, 1)
    lanes = per_group * cap
    meta = jnp.full((GROUPS, 8, lanes), -1.0, F32).at[:, :4, :slots].set(table)

    def by_peer(array):
        return array[0].reshape(tokens, n_sp, cols).transpose(1, 0, 2)

    qkv = jnp.concatenate([by_peer(queries), by_peer(keys_in), by_peer(values_in)], axis=2)
    offsets = (key_shift[0].astype(F32) + head_shift[None, :]).T.reshape(n_sp, heads, tokens)
    offsets = jnp.pad(offsets, ((0, 0), (0, 8 - heads), (0, 0)))
    qkv, offsets = swap(n_sp, 0, qkv, offsets)
    attended = attention(heads, qkv, offsets)
    (attended,) = swap(n_sp, 1, attended)
    att32 = attended.transpose(1, 0, 2).reshape(tokens, n_sp * cols).astype(F32)
    normed = (
        att32 * lax.rsqrt(jnp.mean(att32 * att32, axis=1, keepdims=True) + norm_eps) * mix_gain
    ).astype(BF16)
    mixed = jnp.dot(normed, out_weight, preferred_element_type=F32)
    summed = stream[0].astype(F32) + mixed
    hidden = (
        summed * lax.rsqrt(jnp.mean(summed * summed, axis=1, keepdims=True) + norm_eps) * post_gain
    ).astype(BF16)

    slot_hot = slot_hot.astype(BF16)
    packed = jnp.dot(slot_hot, hidden, preferred_element_type=F32).astype(BF16)
    received, tables = dispatch(n_sp, n_dp, cap, packed.reshape(GROUPS, slots, width), meta)
    rows = received.reshape(GROUPS * per_group * cap, width)
    gate = jnp.dot(rows, w_gate[0], preferred_element_type=F32)
    upper = jnp.dot(rows, w_up[0], preferred_element_type=F32)
    inner = (jax.nn.silu(gate) * upper).astype(BF16)
    reply = jnp.dot(inner, w_down[0], preferred_element_type=F32).astype(BF16)
    returned = combine(n_sp, n_dp, slots, reply.reshape(received.shape), tables)
    moe_sum = lax.dot_general(
        slot_hot,
        returned.reshape(GROUPS * slots, width),
        (((0,), (0,)), ((), ())),
        preferred_element_type=F32,
    )
    return (hidden.astype(F32) + moe_sum).astype(BF16)[None]


def solution(mesh):
    return jax.shard_map(
        functools.partial(on_device, mesh.shape["sp"], mesh.shape["dp"]),
        mesh=mesh,
        in_specs=(
            P("dp", "sp", None),
            P("dp", "sp", None),
            P("dp", "sp", None),
            P("dp", "sp", None),
            P("dp", "sp", None),
            P(),
            P(),
            P(),
            P(),
            P("dp", "sp", None),
            P("dp", "sp", None),
            P(("sp", "dp"), None, None),
            P(("sp", "dp"), None, None),
            P(("sp", "dp"), None, None),
        ),
        out_specs=P("dp", "sp", None),
        check_vma=False,
    )
```

profile of v0, /device:TPU:0, one launch (start us, length us, event | category | flops | bytes accessed | tf_op | source)
XLA Modules:
  0.0 166.1 jit_solution(6372753609826974642)
XLA Ops:
  0.0 0.0 copy-start.1
  0.0 0.7 fusion.33
  0.7 0.8 convert_add_fusion
  1.5 0.6 pad.9.refs_1_
  2.1 0.8 copy.69
  2.9 0.1 eq.54
  3.0 0.2 fusion.13
  3.3 0.1 reduce_sum.53
  3.4 0.1 copy.70
  3.5 0.7 fusion.32
  4.2 0.7 maximum_bitcast_fusion
  4.9 0.2 fusion.14
  5.0 0.7 convert_add_fusion.1
  5.8 0.2 select_reduce_fusion
  6.0 0.1 reduce_sum.55
  6.1 0.7 fusion.25
  6.8 0.6 scatter.4.meta
  7.4 1.1 copy.62
  8.5 0.2 copy.63
  8.7 1.1 copy.64
  9.9 0.2 copy.65
  10.1 0.0 copy-done.1
  10.1 0.2 copy.66
  10.2 0.2 copy.67
  10.4 1.0 pad_maximum_fusion.refs_0_
  11.4 21.6 %swap0.1 = (bf16[8,128,384]{2,1,0:T(8,128)(2,1)}, f32[8,8,128]{2,1,0:T(8,128)}) custom-call(bf16[8,128,384]{2,1,0:T(8,128)(2,1)} %pad_maximum_fusion.refs_0_, f32[8,8,128]{2,1,0:T(8,128)} %pad.9.refs_1_), custom_call_target="tpu_custom_call" | custom-call | tf_op jit(solution)/shard_map/swap0/pallas_call | solution.py:62
  33.0 0.0 copy-start
  33.0 13.4 %attention.1.refs_0_ = bf16[8,128,128]{2,1,0:T(8,128)(2,1)} custom-call(bf16[8,128,384]{2,1,0:T(8,128)(2,1)} %get-tuple-element.21.qkv_ref, f32[8,8,128]{2,1,0:T(8,128)} %get-tuple-element.22.shift_ref), custom_call_target="tpu_custom_call" | custom-call | tf_op jit(solution)/shard_map/attention/pallas_call | solution.py:130
  46.4 15.2 %swap1.1 = bf16[8,128,128]{2,1,0:T(8,128)(2,1)} custom-call(bf16[8,128,128]{2,1,0:T(8,128)(2,1)} %attention.1.refs_0_), custom_call_target="tpu_custom_call" | custom-call | tf_op jit(solution)/shard_map/swap1/pallas_call | solution.py:62
  61.7 1.1 fusion.17
  62.8 1.0 convert_bitcast_fusion
  63.8 0.2 copy.68
  64.0 0.0 copy-done.3
  64.0 0.2 fusion.19
  64.2 0.0 copy-done
  64.2 0.0 copy-start.2
  64.2 0.0 copy-start.4
  64.2 3.2 %multiply_reduce_fusion = (f32[128]{0:T(128)S(1)}, f32[128,2048]{1,0:T(8,128)S(1)}) fusion(bf16[128,1024]{0,1:T(8,128)(2,1)S(1)} %fusion.19, bf16[1024,2048]{1,0:T(8,128)(2,1)} %param.24, bf16[1,128,2048]{2,1,0:T(8,128)(2,1)S(1)} %copy-done), kind=kOutput, calls=%fused_computation.18 | convolution fusion | flops 537919360 | bytes 6029824 | tf_op jit(solution)/shard_map/dot_general | solution.py:446
  67.4 0.0 copy-done.2
  67.4 1.5 convolution_convert_fusion
  68.9 36.9 %dispatch.1 = (bf16[4,8,16,2048]{3,2,1,0:T(8,128)(2,1)}, f32[4,8,128]{2,1,0:T(8,128)}) custom-call(bf16[4,64,2048]{2,1,0:T(8,128)(2,1)} %bitcast.71, f32[4,8,128]{2,1,0:T(8,128)} %scatter.4.meta), custom_call_target="tpu_custom_call" | custom-call | tf_op jit(solution)/shard_map/dispatch/pallas_call | solution.py:252
  105.8 0.0 copy-done.4
  105.8 0.0 copy-start.5
  105.8 5.4 %fusion.4 = f32[512,1024]{1,0:T(8,128)} fusion(bf16[512,2048]{1,0:T(8,128)(2,1)} %bitcast.83, bf16[1,2048,1024]{2,1,0:T(8,128)(2,1)S(1)} %copy-done.4), kind=kOutput, calls=%fused_computation.4 | convolution fusion | flops 2147483648 | bytes 8388608 | tf_op jit(solution)/shard_map/dot_general | solution.py:456
  111.3 0.0 copy-done.5
  111.3 9.9 %fusion.6 = bf16[512,2048]{1,0:T(8,128)(2,1)} fusion(bf16[1,1024,2048]{2,1,0:T(8,128)(2,1)} %param.30, f32[512,1024]{1,0:T(8,128)} %fusion.4, bf16[512,2048]{1,0:T(8,128)(2,1)S(1)} %bitcast.84, bf16[1,2048,1024]{2,1,0:T(8,128)(2,1)} %param.29), kind=kOutput, calls=%fused_computation.6 | convolution fusion | flops 4299161600 | bytes 14680064 | tf_op jit(solution)/shard_map/dot_general | solution.py:459
  121.2 42.5 %combine.1 = bf16[4,64,2048]{2,1,0:T(8,128)(2,1)} custom-call(bf16[4,8,16,2048]{3,2,1,0:T(8,128)(2,1)} %bitcast.72, f32[4,8,128]{2,1,0:T(8,128)} %get-tuple-element.24.meta), custom_call_target="tpu_custom_call" | custom-call | tf_op jit(solution)/shard_map/combine/pallas_call | solution.py:362
  163.8 2.4 %fusion.10 = bf16[1,128,2048]{2,1,0:T(8,128)(2,1)} fusion(bf16[256,2048]{1,0:T(8,128)(2,1)} %bitcast.70, s32[128]{0:T(128)S(1)} %convert_add_fusion.1, f32[2048]{0:T(1024)S(1)} %copy-done.2, f32[128,2048]{1,0:T(8,128)S(1)} %get-tuple-element.26, f32[128]{0:T(128)S(1)} %add_rsqrt_fusion), kind=kOutput, calls=%fused_computation.11 | convolution fusion | flops 135823360 | bytes 2630656 | tf_op jit(solution)/shard_map/dot_general | solution.py:461
  (5 shorter events, 0.1 us)
Async XLA Ops:
  0.0 10.1 %copy-start.1 = (bf16[1,128,1024]{2,1,0:T(8,128)(2,1)S(1)}, bf16[1,128,1024]{2,1,0:T(8,128)(2,1)}, u32[]{:S(2)}) copy-start(bf16[1,128,1024]{2,1,0:T(8,128)(2,1)} %param.20) | copy-start | bytes 786436
  11.4 52.6 %copy-start.3 = (f32[1024]{0:T(1024)S(1)}, f32[1024]{0:T(1024)}, u32[]{:S(2)}) copy-start(f32[1024]{0:T(1024)} %param.23) | copy-start | bytes 12292
  33.0 31.2 %copy-start = (bf16[1,128,2048]{2,1,0:T(8,128)(2,1)S(1)}, bf16[1,128,2048]{2,1,0:T(8,128)(2,1)}, u32[]{:S(2)}) copy-start(bf16[1,128,2048]{2,1,0:T(8,128)(2,1)} %param.17) | copy-start | bytes 1572868
  64.2 3.2 %copy-start.2 = (f32[2048]{0:T(1024)S(1)}, f32[2048]{0:T(1024)}, u32[]{:S(2)}) copy-start(f32[2048]{0:T(1024)} %param.25) | copy-start | bytes 24580
  64.2 41.6 %copy-start.4 = (bf16[1,2048,1024]{2,1,0:T(8,128)(2,1)S(1)}, bf16[1,2048,1024]{2,1,0:T(8,128)(2,1)}, u32[]{:S(2)}) copy-start(bf16[1,2048,1024]{2,1,0:T(8,128)(2,1)} %param.28) | copy-start | bytes 12582916
  105.8 5.5 %copy-start.5 = (bf16[4,8,16,2048]{3,2,1,0:T(8,128)(2,1)S(1)}, bf16[4,8,16,2048]{3,2,1,0:T(8,128)(2,1)}, u32[]{:S(2)}) copy-start(bf16[4,8,16,2048]{3,2,1,0:T(8,128)(2,1)} %get-tuple-element.23) | copy-start | bytes 6291460
where the time goes:
time: 167 us; the launch traced here: 166 us
  Pallas kernels  130 us (78%)
  matrix products  22.8 us (14%)
  other arithmetic  7.88 us (5%)
  local copies, waits for them, and re-layouts  5.62 us (3%)
    pallas_call x1, Pallas kernels, combine(): pl.pallas_call(functools.partial(combine_kernel, n_sp, n_dp), out_shape=j...  42.5 us
    pallas_call x1, Pallas kernels, dispatch(): pl.pallas_call(functools.partial(dispatch_kernel, n_sp, n_dp), out_shape=...  36.9 us
    pallas_call x2, Pallas kernels, swap(): pl.pallas_call(functools.partial(swap_kernel, n, count), out_shape=[jax.S...  36.8 us
    pallas_call x1, Pallas kernels, attention(): pl.pallas_call(functools.partial(attention_kernel, heads), out_shape=jax....  13.4 us
    dot_general x1, matrix products, on_device(): reply = jnp.dot(inner, w_down[0], preferred_element_type=F32).astype(BF16)  9.95 us
    dot_general x1, matrix products, on_device(): gate = jnp.dot(rows, w_gate[0], preferred_element_type=F32)  5.44 us

commit v1 on v0

--- a/solution.py
+++ b/solution.py
@@ -167,217 +167,270 @@
     return lanes == meta[row : row + 1, :]
 
 
-def dispatch_kernel(
+def moe_kernel(
     n_sp,
     n_dp,
+    hidden,
+    slot_hot,
+    token_hot,
+    meta,
+    gate_hbm,
+    up_hbm,
+    down_hbm,
+    result,
     packed,
-    meta,
+    landed,
+    tables,
+    stage,
     got,
-    got_meta,
-    block,
-    stage,
+    inner,
+    reply,
+    back,
+    partial,
+    returned,
+    gate_w,
+    up_w,
+    down_w,
+    w_sem,
+    t_send,
+    t_recv,
     z_send,
     z_recv,
-    t_send,
-    t_recv,
     p_send,
     p_recv,
-    own_sem,
+    r_send,
+    r_recv,
+    y_send,
+    y_recv,
 ):
-    _, per_group, cap, width = got.shape
+    tokens, width = hidden.shape
+    _, per_group, cap, _ = got.shape
     slots = packed.shape[1]
+    lanes = per_group * cap
+    ffn = inner.shape[1]
     chunk = min(512, width)
+    chunks = [pl.ds(c, chunk) for c in range(0, width, chunk)]
     plane, member, at = place(n_sp, n_dp)
+
+    loads = [
+        pltpu.make_async_copy(gate_hbm, gate_w, w_sem.at[0]),
+        pltpu.make_async_copy(up_hbm, up_w, w_sem.at[1]),
+        pltpu.make_async_copy(down_hbm, down_w, w_sem.at[2]),
+    ]
+    for load in loads:
+        load.start()
     greet(plane, member, at, per_group)
-    z_copies, t_copies = [None], [None]
-    for d in range(1, GROUPS):
-        other = lax.rem(plane + d, GROUPS)
-        for kept, src, dst, send, recv in (
-            (t_copies, meta, got_meta, t_send, t_recv),
-            (z_copies, packed, block, z_send, z_recv),
-        ):
-            kept.append(
-                pltpu.make_async_remote_copy(
-                    src_ref=src.at[other],
-                    dst_ref=dst.at[plane],
-                    send_sem=send.at[d],
-                    recv_sem=recv.at[d],
-                    device_id=at(other, member),
-                    device_id_type=MESH,
-                )
+
+    flip = 1 - 2 * lax.rem(plane, 2)
+    others = [plane, plane + flip, lax.rem(plane + 2, GROUPS), GROUPS - 1 - plane]
+
+    def put_rows(ref, source, cols, rows):
+        if cap % 16 == 0:
+            ref[source, :, :, cols] = rows.astype(BF16).reshape(per_group, cap, chunk)
+        else:
+            for m in range(per_group):
+                ref[source, m, :, cols] = rows[m * cap : (m + 1) * cap].astype(BF16)
+
+    def take_rows(ref, source, cols):
+        if cap % 16 == 0:
+            rows = ref[source, :, :, cols]
+            return rows.reshape(lanes, rows.shape[-1])
+        return jnp.concatenate(
+            [ref[source, m, :, cols].astype(F32) for m in range(per_group)], axis=0
+        ).astype(BF16)
+
+    sends = []
+
+    def remote(src, dst, send, recv, device):
+        copy = pltpu.make_async_remote_copy(
+            src_ref=src,
+            dst_ref=dst,
+            send_sem=send,
+            recv_sem=recv,
+            device_id=device,
+            device_id_type=MESH,
+        )
+        copy.start()
+        return copy
+
+    z_copies = {}
+    for k in range(1, GROUPS):
+        q = others[k]
+        z_copies[k, -1] = remote(
+            meta.at[q], tables.at[plane], t_send.at[k], t_recv.at[k], at(q, member)
+        )
+        hot = slot_hot[q]
+        for c, cols in enumerate(chunks):
+            packed[q, :, cols] = jnp.dot(
+                hot, hidden[:, cols], preferred_element_type=F32
+            ).astype(BF16)
+            z_copies[k, c] = remote(
+                packed.at[q, :, cols],
+                landed.at[plane, :, cols],
+                z_send.at[k, c],
+                z_recv.at[k, c],
+                at(q, member),
             )
-            kept[-1].start()
-    got_meta[plane] = meta[plane]
-    later = []
-    for d in range(GROUPS):
-        source = lax.rem(plane - d + GROUPS, GROUPS)
-        if d:
-            t_copies[d].wait_recv()
-            z_copies[d].wait_recv()
-        held = block if d else packed
-        info = got_meta[source]
+    tables[plane] = meta[plane]
+    hot = slot_hot[plane]
+    for cols in chunks:
+        landed[plane, :, cols] = jnp.dot(
+            hot, hidden[:, cols], preferred_element_type=F32
+        ).astype(BF16)
+
+    def fan_out(source, src, dst, cols, send, recv):
+        for e in range(1, per_group):
+            other = lax.rem(member + e, per_group)
+            remote(
+                src.at[source, other, :, cols],
+                dst.at[source, member, :, cols],
+                send,
+                recv,
+                at(plane, other),
+            )
+        dst[source, member, :, cols] = src[source, member, :, cols]
+
+    def group_wait(source, ref, cols, sem):
+        part = ref.at[source, pl.ds(0, per_group - 1), :, cols]
+        pltpu.make_async_copy(part, part, sem).wait()
+
+    def deliver(k):
+        source = others[k]
+        if k:
+            z_copies[k, -1].wait_recv()
+        info = tables[source]
         hot = jnp.where(one_hot_rows(info, 0) | one_hot_rows(info, 1), 1.0, 0.0).astype(BF16)
         hot = hot[:, :slots]
-        for c in range(0, width, chunk):
-            rows = jnp.dot(hot, held[source, :, c : c + chunk], preferred_element_type=F32)
-            for m in range(per_group):
-                stage[source, m, :, c : c + chunk] = rows[m * cap : (m + 1) * cap].astype(BF16)
-        own = pltpu.make_async_copy(stage.at[source, member], got.at[source, member], own_sem.at[d])
-        own.start()
-        later.append(own)
-        for e in range(1, per_group):
-            other = lax.rem(member + e, per_group)
-            copy = pltpu.make_async_remote_copy(
-                src_ref=stage.at[source, other],
-                dst_ref=got.at[source, member],
-                send_sem=p_send.at[d, e],
-                recv_sem=p_recv.at[d, e],
-                device_id=at(plane, other),
-                device_id_type=MESH,
+        for c, cols in enumerate(chunks):
+            if k:
+                z_copies[k, c].wait_recv()
+            rows = jnp.dot(hot, landed[source, :, cols], preferred_element_type=F32)
+            put_rows(stage, source, cols, rows)
+            fan_out(source, stage, got, cols, p_send.at[k, c], p_recv.at[k, c])
+
+    def experts(k):
+        source = others[k]
+        for c, cols in enumerate(chunks):
+            group_wait(source, got, cols, p_recv.at[k, c])
+        if k == 0:
+            for load in loads:
+                load.wait()
+        rows = take_rows(got, source, slice(None))
+        part = min(256, ffn)
+        for n in range(0, ffn, part):
+            gate = jnp.dot(rows, gate_w[:, n : n + part], preferred_element_type=F32)
+            upper = jnp.dot(rows, up_w[:, n : n + part], preferred_element_type=F32)
+            inner[:, n : n + part] = (gate / (1.0 + jnp.exp(-gate)) * upper).astype(BF16)
+        for c, cols in enumerate(chunks):
+            out = jnp.dot(inner[...], down_w[:, cols], preferred_element_type=F32)
+            put_rows(reply, source, cols, out)
+            fan_out(source, reply, back, cols, r_send.at[k, c], r_recv.at[k, c])
+
+    y_copies = {}
+
+    def combine(k):
+        source = others[k]
+        info = tables[source]
+        spread = jnp.where(one_hot_rows(info, 0), info[2:3, :], 0.0) + jnp.where(
+            one_hot_rows(info, 1), info[3:4, :], 0.0
+        )
+        spread = spread.T[:slots]
+        high = spread.astype(BF16)
+        low = (spread - high.astype(F32)).astype(BF16)
+        for c, cols in enumerate(chunks):
+            group_wait(source, back, cols, r_recv.at[k, c])
+            rows = take_rows(back, source, cols)
+            total = jnp.dot(high, rows, preferred_element_type=F32) + jnp.dot(
+                low, rows, preferred_element_type=F32
             )
-            copy.start()
-            later.append(copy)
-    for copy in later:
-        copy.wait()
-    for d in range(1, GROUPS):
-        t_copies[d].wait_send()
-        z_copies[d].wait_send()
-
-
-def dispatch(n_sp, n_dp, cap, packed, meta):
+            if k:
+                partial[source, :, cols] = total.astype(BF16)
+                y_copies[k, c] = remote(
+                    partial.at[source, :, cols],
+                    returned.at[plane, :, cols],
+                    y_send.at[k, c],
+                    y_recv.at[k, c],
+                    at(source, member),
+                )
+            else:
+                returned[source, :, cols] = total.astype(BF16)
+
+    deliver(0)
+    deliver(1)
+    experts(0)
+    deliver(2)
+    experts(1)
+    deliver(3)
+    experts(2)
+    combine(1)
+    experts(3)
+    combine(2)
+    combine(0)
+    combine(3)
+
+    for c, cols in enumerate(chunks):
+        for k in range(1, GROUPS):
+            y_copies[k, c].wait_recv()
+        rows = returned[:, :, cols].reshape(GROUPS * slots, chunk)
+        total = jnp.dot(token_hot[...], rows, preferred_element_type=F32)
+        result[:, cols] = (hidden[:, cols].astype(F32) + total).astype(BF16)
+
+    for k in range(GROUPS):
+        for c, cols in enumerate(chunks):
+            if k:
+                z_copies[k, c].wait_send()
+                y_copies[k, c].wait_send()
+            group_wait(others[k], stage, cols, p_send.at[k, c])
+            group_wait(others[k], reply, cols, r_send.at[k, c])
+        if k:
+            z_copies[k, -1].wait_send()
+
+
+def moe(n_sp, n_dp, cap, hidden, slot_hot, token_hot, meta, w_gate, w_up, w_down):
     per_group = n_sp * n_dp // GROUPS
-    _, slots, width = packed.shape
-    buffer = (GROUPS, per_group, cap, width)
+    tokens, width = hidden.shape
+    slots = slot_hot.shape[1]
+    ffn = w_gate.shape[1]
+    chunks = width // min(512, width)
     dma = pltpu.SemaphoreType.DMA
+    wide = (GROUPS, per_group, cap, width)
+    narrow = (GROUPS, slots, width)
     return pl.pallas_call(
-        functools.partial(dispatch_kernel, n_sp, n_dp),
-        out_shape=[
-            jax.ShapeDtypeStruct(buffer, BF16),
-            jax.ShapeDtypeStruct(meta.shape, F32),
-        ],
-        in_specs=vmem(2),
-        out_specs=vmem(2),
+        functools.partial(moe_kernel, n_sp, n_dp),
+        out_shape=jax.ShapeDtypeStruct((tokens, width), BF16),
+        in_specs=vmem(4) + [pl.BlockSpec(memory_space=pl.ANY)] * 3,
+        out_specs=vmem(1)[0],
         scratch_shapes=[
-            pltpu.VMEM(packed.shape, BF16),
-            pltpu.VMEM(buffer, BF16),
+            pltpu.VMEM(narrow, BF16),
+            pltpu.VMEM(narrow, BF16),
+            pltpu.VMEM(meta.shape, F32),
+            pltpu.VMEM(wide, BF16),
+            pltpu.VMEM(wide, BF16),
+            pltpu.VMEM((per_group * cap, ffn), BF16),
+            pltpu.VMEM(wide, BF16),
+            pltpu.VMEM(wide, BF16),
+            pltpu.VMEM(narrow, BF16),
+            pltpu.VMEM(narrow, BF16),
+            pltpu.VMEM(w_gate.shape, BF16),
+            pltpu.VMEM(w_up.shape, BF16),
+            pltpu.VMEM(w_down.shape, BF16),
+            dma((3,)),
             dma((GROUPS,)),
             dma((GROUPS,)),
-            dma((GROUPS,)),
-            dma((GROUPS,)),
-            dma((GROUPS, per_group)),
-            dma((GROUPS, per_group)),
-            dma((GROUPS,)),
+            dma((GROUPS, chunks)),
+            dma((GROUPS, chunks)),
+            dma((GROUPS, chunks)),
+            dma((GROUPS, chunks)),
+            dma((GROUPS, chunks)),
+            dma((GROUPS, chunks)),
+            dma((GROUPS, chunks)),
+            dma((GROUPS, chunks)),
         ],
         compiler_params=pltpu.CompilerParams(
             collective_id=2, has_side_effects=True, vmem_limit_bytes=VLIM
         ),
-        name="dispatch",
-    )(packed, meta)
-
-
-def combine_kernel(
-    n_sp,
-    n_dp,
-    reply,
-    meta,
-    out,
-    block,
-    stage,
-    z_send,
-    z_recv,
-    p_send,
-    p_recv,
-    own_sem,
-):
-    _, per_group, cap, width = reply.shape
-    slots = out.shape[1]
-    chunk = min(512, width)
-    plane, member, at = place(n_sp, n_dp)
-    greet(plane, member, at, per_group)
-    order = list(range(1, GROUPS)) + [0]
-    plane_copies = {}
-    for d in order:
-        target = lax.rem(plane + d, GROUPS)
-        own = pltpu.make_async_copy(reply.at[target, member], block.at[target, member], own_sem.at[d])
-        own.start()
-        copies = [own]
-        for e in range(1, per_group):
-            other = lax.rem(member + e, per_group)
-            copies.append(
-                pltpu.make_async_remote_copy(
-                    src_ref=reply.at[target, other],
-                    dst_ref=block.at[target, member],
-                    send_sem=p_send.at[d, e],
-                    recv_sem=p_recv.at[d, e],
-                    device_id=at(plane, other),
-                    device_id_type=MESH,
-                )
-            )
-            copies[-1].start()
-        plane_copies[d] = copies
-    z_copies = []
-    for d in order:
-        target = lax.rem(plane + d, GROUPS)
-        for copy in plane_copies[d]:
-            copy.wait()
-        info = meta[target]
-        spread = jnp.where(one_hot_rows(info, 0), info[2:3, :], 0.0) + jnp.where(
-            one_hot_rows(info, 1), info[3:4, :], 0.0
-        )
-        spread = spread.T[:slots]
-        high = spread.astype(BF16)
-        low = (spread - high.astype(F32)).astype(BF16)
-        for c in range(0, width, chunk):
-            if cap % 16 == 0:
-                rows = block[target, :, :, c : c + chunk].reshape(per_group * cap, chunk)
-            else:
-                rows = jnp.concatenate(
-                    [block[target, m, :, c : c + chunk].astype(F32) for m in range(per_group)], axis=0
-                ).astype(BF16)
-            total = jnp.dot(high, rows, preferred_element_type=F32) + jnp.dot(
-                low, rows, preferred_element_type=F32
-            )
-            if d:
-                stage[target, :, c : c + chunk] = total.astype(BF16)
-            else:
-                out[target, :, c : c + chunk] = total.astype(BF16)
-        if d:
-            copy = pltpu.make_async_remote_copy(
-                src_ref=stage.at[target],
-                dst_ref=out.at[plane],
-                send_sem=z_send.at[d],
-                recv_sem=z_recv.at[d],
-                device_id=at(target, member),
-                device_id_type=MESH,
-            )
-            copy.start()
-            z_copies.append(copy)
-    for copy in z_copies:
-        copy.wait()
-
-
-def combine(n_sp, n_dp, slots, reply, meta):
-    _, per_group, cap, width = reply.shape
-    dma = pltpu.SemaphoreType.DMA
-    return pl.pallas_call(
-        functools.partial(combine_kernel, n_sp, n_dp),
-        out_shape=jax.ShapeDtypeStruct((GROUPS, slots, width), BF16),
-        in_specs=vmem(2),
-        out_specs=vmem(1)[0],
-        scratch_shapes=[
-            pltpu.VMEM(reply.shape, BF16),
-            pltpu.VMEM((GROUPS, slots, width), BF16),
-            dma((GROUPS,)),
-            dma((GROUPS,)),
-            dma((GROUPS, per_group)),
-            dma((GROUPS, per_group)),
-            dma((GROUPS,)),
-        ],
-        compiler_params=pltpu.CompilerParams(
-            collective_id=3, has_side_effects=True, vmem_limit_bytes=VLIM
-        ),
-        name="combine",
-    )(reply, meta)
+        name="moe",
+    )(hidden, slot_hot, token_hot, meta, w_gate, w_up, w_down)
 
 
 def on_device(
@@ -450,21 +503,19 @@
     ).astype(BF16)
 
     slot_hot = slot_hot.astype(BF16)
-    packed = jnp.dot(slot_hot, hidden, preferred_element_type=F32).astype(BF16)
-    received, tables = dispatch(n_sp, n_dp, cap, packed.reshape(GROUPS, slots, width), meta)
-    rows = received.reshape(GROUPS * per_group * cap, width)
-    gate = jnp.dot(rows, w_gate[0], preferred_element_type=F32)
-    upper = jnp.dot(rows, w_up[0], preferred_element_type=F32)
-    inner = (jax.nn.silu(gate) * upper).astype(BF16)
-    reply = jnp.dot(inner, w_down[0], preferred_element_type=F32).astype(BF16)
-    returned = combine(n_sp, n_dp, slots, reply.reshape(received.shape), tables)
-    moe_sum = lax.dot_general(
-        slot_hot,
-        returned.reshape(GROUPS * slots, width),
-        (((0,), (0,)), ((), ())),
-        preferred_element_type=F32,
+    out = moe(
+        n_sp,
+        n_dp,
+        cap,
+        hidden,
+        slot_hot.reshape(GROUPS, slots, tokens),
+        slot_hot.T,
+        meta,
+        w_gate[0],
+        w_up[0],
+        w_down[0],
     )
-    return (hidden.astype(F32) + moe_sum).astype(BF16)[None]
+    return out[None]
 
 
 def solution(mesh):

time: 167 us -> 137 us (0.82)
  the two profiles are of different devices: /device:TPU:0 before, /device:TPU:13 now
where the time goes in v1:
time: 137 us
  Pallas kernels  119 us (87%)
  local copies, waits for them, and re-layouts  7.82 us (6%)
  other arithmetic  6.14 us (4%)
  matrix products  3.38 us (2%)
    pallas_call x1, Pallas kernels, moe(): pl.pallas_call(functools.partial(moe_kernel, n_sp, n_dp), out_shape=jax.S...  71.6 us
    pallas_call x2, Pallas kernels, swap(): pl.pallas_call(functools.partial(swap_kernel, n, count), out_shape=[jax.S...  34.4 us
    pallas_call x1, Pallas kernels, attention(): pl.pallas_call(functools.partial(attention_kernel, heads), out_shape=jax....  13.4 us
    unnamed x21, local copies, waits for them, and re-layouts  5.43 us
    dot_general x1, matrix products, on_device(): mixed = jnp.dot(normed, out_weight, preferred_element_type=F32)  3.02 us

profile of v1, /device:TPU:13, one launch (start us, length us, event | category | flops | bytes accessed | tf_op | source)
XLA Modules:
  0.0 137.0 jit_solution(1348592887593195129)
XLA Ops:
  0.0 0.0 copy-start.4
  0.0 0.0 copy-start.6
  0.0 1.1 copy.62
  1.2 0.2 copy.63
  1.3 0.0 copy-start.2
  1.4 1.1 copy.64
  2.5 0.0 copy-start
  2.5 0.2 copy.65
  2.7 1.1 copy.66
  3.8 0.2 copy.67
  4.0 1.0 pad_maximum_fusion.refs_0_
  5.0 0.0 copy-done.4
  5.0 0.0 copy-done.6
  5.0 0.1 convert_add_fusion
  5.1 0.6 pad.9.refs_1_
  5.7 24.6 %swap0.1 = (bf16[8,128,384]{2,1,0:T(8,128)(2,1)}, f32[8,8,128]{2,1,0:T(8,128)}) custom-call(bf16[8,128,384]{2,1,0:T(8,128)(2,1)} %pad_maximum_fusion.refs_0_, f32[8,8,128]{2,1,0:T(8,128)} %pad.9.refs_1_), custom_call_target="tpu_custom_call" | custom-call | tf_op jit(solution)/shard_map/swap0/pallas_call | solution.py:62
  30.3 13.4 %attention.1.refs_0_ = bf16[8,128,128]{2,1,0:T(8,128)(2,1)} custom-call(bf16[8,128,384]{2,1,0:T(8,128)(2,1)} %get-tuple-element.19.qkv_ref, f32[8,8,128]{2,1,0:T(8,128)} %get-tuple-element.20.shift_ref), custom_call_target="tpu_custom_call" | custom-call | tf_op jit(solution)/shard_map/attention/pallas_call | solution.py:130
  43.7 9.9 %swap1.1 = bf16[8,128,128]{2,1,0:T(8,128)(2,1)} custom-call(bf16[8,128,128]{2,1,0:T(8,128)(2,1)} %attention.1.refs_0_), custom_call_target="tpu_custom_call" | custom-call | tf_op jit(solution)/shard_map/swap1/pallas_call | solution.py:62
  53.5 1.0 convert_bitcast_fusion
  54.5 0.0 copy-start.1
  54.5 0.2 copy.68
  54.7 1.1 fusion.2
  55.8 0.0 copy-done.2
  55.8 0.0 copy-start.3
  55.9 0.2 fusion.4
  56.1 0.0 copy-done
  56.1 0.0 copy-start.5
  56.1 0.0 copy-start.7
  56.1 3.0 %multiply_reduce_fusion = (f32[128]{0:T(128)S(1)}, f32[128,2048]{1,0:T(8,128)S(1)}) fusion(bf16[128,1024]{0,1:T(8,128)(2,1)S(1)} %fusion.4, bf16[1024,2048]{1,0:T(8,128)(2,1)} %param.24, bf16[1,128,2048]{2,1,0:T(8,128)(2,1)S(1)} %copy-done), kind=kOutput, calls=%fused_computation.6 | convolution fusion | flops 537919360 | bytes 6029824 | tf_op jit(solution)/shard_map/dot_general | solution.py:499
  59.1 0.0 copy-done.1
  59.1 1.0 multiply_convert_fusion.hidden
  60.1 0.0 copy-done.3
  60.1 0.2 fusion.1
  60.4 0.1 copy.69
  60.5 0.1 eq.83
  60.6 0.2 fusion
  60.8 0.1 reduce_sum.53
  61.0 0.1 copy.70
  61.1 0.0 copy-done.5
  61.1 0.2 select_reduce_fusion
  61.3 0.1 reduce_sum.55
  61.4 0.0 copy-done.7
  61.4 0.1 fusion.9
  61.5 0.6 scatter.4.meta
  62.1 0.7 compare_convert_fusion.slot_hot
  62.8 0.7 fusion.5.token_hot
  63.5 71.6 %moe.1 = bf16[128,2048]{1,0:T(8,128)(2,1)} custom-call(bf16[128,2048]{1,0:T(8,128)(2,1)} %multiply_convert_fusion.hidden, bf16[4,64,128]{2,1,0:T(8,128)(2,1)} %compare_convert_fusion.slot_hot, bf16[128,256]{1,0:T(8,128)(2,1)} %fusion.5.token_hot, f32[4,8,128]{2,1,0:T(8,128)} %scatter.4.meta, bf16[2048,1024]{1,0:T(8,128)(2,1)} %bitcast.50, ...), custom_call_target="tpu_custom_call" | custom-call | tf_op jit(solution)/shard_map/moe/pallas_call | solution.py:398
  135.1 1.9 %copy.77 = bf16[1,128,2048]{2,1,0:T(8,128)(2,1)} copy(bf16[1,128,2048]{2,1,0:T(8,128)(2,1)} %bitcast.53) | data formatting | bytes 1048576
  (9 shorter events, 0.1 us)
Async XLA Ops:
  0.0 5.0 %copy-start.4 = (bf16[1,128,16]{1,2,0:T(8,128)(2,1)S(1)}, bf16[1,128,16]{1,2,0:T(8,128)(2,1)}, u32[]{:S(2)}) copy-start(bf16[1,128,16]{1,2,0:T(8,128)(2,1)} %param.21) | copy-start | bytes 12292
  0.0 5.0 %copy-start.6 = (f32[16]{0:T(128)S(1)}, f32[16]{0:T(128)}, u32[]{:S(2)}) copy-start(f32[16]{0:T(128)} %param.22) | copy-start | bytes 196
  1.3 54.5 %copy-start.2 = (f32[1024]{0:T(1024)S(1)}, f32[1024]{0:T(1024)}, u32[]{:S(2)}) copy-start(f32[1024]{0:T(1024)} %param.23) | copy-start | bytes 12292
  2.5 53.6 %copy-start = (bf16[1,128,2048]{2,1,0:T(8,128)(2,1)S(1)}, bf16[1,128,2048]{2,1,0:T(8,128)(2,1)}, u32[]{:S(2)}) copy-start(bf16[1,128,2048]{2,1,0:T(8,128)(2,1)} %param.17) | copy-start | bytes 1572868
  54.5 4.6 %copy-start.1 = (f32[2048]{0:T(1024)S(1)}, f32[2048]{0:T(1024)}, u32[]{:S(2)}) copy-start(f32[2048]{0:T(1024)} %param.25) | copy-start | bytes 24580
  55.8 4.2 %copy-start.3 = (s32[1,128,2]{1,2,0:T(2,128)S(1)}, s32[1,128,2]{1,2,0:T(2,128)}, u32[]{:S(2)}) copy-start(s32[1,128,2]{1,2,0:T(2,128)} %param.26) | copy-start | bytes 3076
  56.1 5.0 %copy-start.5 = (f32[1,128,2]{1,2,0:T(2,128)S(1)}, f32[1,128,2]{1,2,0:T(2,128)}, u32[]{:S(2)}) copy-start(f32[1,128,2]{1,2,0:T(2,128)} %param.27) | copy-start | bytes 3076
  56.1 5.3 %copy-start.7 = (f32[4]{0:T(128)S(1)}, f32[4]{0:T(128)}, u32[]{:S(2)}) copy-start(f32[4]{0:T(128)} %constant.85) | copy-start | bytes 52

commit v2 on v1

v2 whole, which is shorter than its diff:
```python
import functools
import math

import jax
import jax.numpy as jnp
from jax import lax
from jax.experimental import pallas as pl
from jax.experimental.pallas import tpu as pltpu
from jax.sharding import PartitionSpec as P

HD = 64
GROUPS = 4
MESH = pl.DeviceIdType.MESH
F32 = jnp.float32
BF16 = jnp.bfloat16
VLIM = 60 * 1024 * 1024
LOG2E = math.log2(math.e)

norm_eps = 1e-05


def one_hot_rows(meta, row):
    lanes = lax.broadcasted_iota(jnp.int32, (meta.shape[1], meta.shape[1]), 0).astype(F32)
    return lanes == meta[row : row + 1, :]


def ones_where(mask):
    return jnp.where(mask, 1.0, 0.0).astype(BF16)


def layer_kernel(
    n_sp,
    n_dp,
    queries,
    keys_in,
    values_in,
    key_shift,
    head_shift,
    mix_gain,
    out_hbm,
    post_gain,
    stream_hbm,
    route,
    route_weight,
    gate_hbm,
    up_hbm,
    down_hbm,
    result,
    q_own,
    k_own,
    v_own,
    outbox,
    inbox,
    shift_pad,
    shift_out,
    shift_in,
    q_all,
    k_all,
    v_all,
    att_out,
    att_in,
    att,
    stream,
    summed,
    hidden,
    meta,
    slot_hot,
    token_hot,
    packed,
    landed,
    tables,
    stage,
    got,
    inner,
    reply,
    back,
    partial,
    returned,
    out_w,
    gate_w,
    up_w,
    down_w,
    i_sem,
    w_sem,
    s_send,
    s_recv,
    q_send,
    q_recv,
    a_send,
    a_recv,
    t_send,
    t_recv,
    z_send,
    z_recv,
    p_send,
    p_recv,
    r_send,
    r_recv,
    y_send,
    y_recv,
):
    tokens, width = hidden.shape
    heads = inbox.shape[0]
    half = tokens // 2
    _, per_group, cap, _ = got.shape
    slots = packed.shape[1]
    lanes = per_group * cap
    ffn = inner.shape[1]
    chunk = min(512, width)
    chunks = [pl.ds(c, chunk) for c in range(0, width, chunk)]
    me, dp = lax.axis_index("sp"), lax.axis_index("dp")
    ny = n_sp // GROUPS
    plane, y = me // ny, lax.rem(me, ny)
    member = y * n_dp + dp
    flip = 1 - 2 * lax.rem(plane, 2)
    others = [plane, plane + flip, lax.rem(plane + 2, GROUPS), GROUPS - 1 - plane]

    def at(g, m):
        return (g * ny + m // n_dp, lax.rem(m, n_dp))

    def remote(src, dst, send, recv, device):
        copy = pltpu.make_async_remote_copy(
            src_ref=src,
            dst_ref=dst,
            send_sem=send,
            recv_sem=recv,
            device_id=device,
            device_id_type=MESH,
        )
        copy.start()
        return copy

    def settle(part, sem):
        pltpu.make_async_copy(part, part, sem).wait()

    qkv_loads = [
        pltpu.make_async_copy(queries, q_own, i_sem.at[0]),
        pltpu.make_async_copy(keys_in, k_own, i_sem.at[1]),
        pltpu.make_async_copy(values_in, v_own, i_sem.at[2]),
    ]
    for load in qkv_loads:
        load.start()
    barrier = pltpu.get_barrier_semaphore()
    for d in range(1, n_sp):
        pl.semaphore_signal(
            barrier, inc=1, device_id=(lax.rem(me + d, n_sp), dp), device_id_type=MESH
        )
    for d in range(1, n_dp):
        for row in range(ny):
            pl.semaphore_signal(
                barrier,
                inc=1,
                device_id=(plane * ny + row, lax.rem(dp + d, n_dp)),
                device_id_type=MESH,
            )

    n_heads = key_shift.shape[1]
    shift_pad[...] = jnp.zeros_like(shift_pad)
    shift_pad[:, :n_heads] = (key_shift[...].astype(F32) + head_shift[...]) * LOG2E
    turned = shift_pad[...].T
    for p in range(n_sp):
        shift_out[p, :heads, :] = turned[p * heads : (p + 1) * heads]
    shift_in[me] = shift_out[me]

    for load in qkv_loads:
        load.wait()
    weight_loads = [
        pltpu.make_async_copy(stream_hbm, stream, w_sem.at[0]),
        pltpu.make_async_copy(out_hbm, out_w, w_sem.at[1]),
        pltpu.make_async_copy(gate_hbm, gate_w, w_sem.at[2]),
        pltpu.make_async_copy(up_hbm, up_w, w_sem.at[3]),
        pltpu.make_async_copy(down_hbm, down_w, w_sem.at[4]),
    ]
    for load in weight_loads:
        load.start()

    def pack_head(h):
        for p in range(n_sp):
            g = p * heads + h
            cols = slice(g * HD, (g + 1) * HD)
            outbox[h, p, :tokens, :] = jnp.concatenate([q_own[:, cols], k_own[:, cols]], axis=1)
            outbox[h, p, tokens:, :] = jnp.concatenate(
                [v_own[:half, cols], v_own[half:, cols]], axis=1
            )
        inbox[h, me] = outbox[h, me]

    order = sorted(range(1, n_sp), key=lambda d: abs(2 * d - n_sp))

    def send_head(h):
        for d in order:
            peer = lax.rem(me + d, n_sp)
            remote(
                outbox.at[h, peer], inbox.at[h, me], q_send.at[h], q_recv.at[h], (peer, dp)
            )

    pack_head(0)
    pl.semaphore_wait(barrier, n_sp - 1 + (n_dp - 1) * ny)
    for d in order:
        peer = lax.rem(me + d, n_sp)
        remote(shift_out.at[peer], shift_in.at[me], s_send.at[0], s_recv.at[0], (peer, dp))
    send_head(0)
    for h in range(1, heads):
        pack_head(h)
        send_head(h)

    row = lax.broadcasted_iota(jnp.int32, (tokens, tokens), 0)
    col = lax.broadcasted_iota(jnp.int32, (tokens, tokens), 1)
    earlier = ones_where(row > col)
    n_expert = n_sp * n_dp
    wide = max(tokens, n_expert)
    expert = lax.broadcasted_iota(jnp.int32, (tokens, wide), 1)
    first, second = route[:, 0:1], route[:, 1:2]
    hit0, hit1 = first == expert, second == expert
    count0 = jnp.dot(earlier, ones_where(hit0), preferred_element_type=F32)
    count1 = jnp.dot(earlier, ones_where(hit1), preferred_element_type=F32) + jnp.dot(
        jnp.ones((tokens, tokens), BF16), ones_where(hit0), preferred_element_type=F32
    )
    rank0 = jnp.sum(jnp.where(hit0, count0, 0.0), axis=1, keepdims=True)
    rank1 = jnp.sum(jnp.where(hit1, count1, 0.0), axis=1, keepdims=True)
    group = jnp.zeros((tokens, 1), F32)
    for g in range(1, GROUPS):
        group = group + jnp.where(first >= g * per_group, 1.0, 0.0)
    lane = col.astype(F32)
    in_group = lane == group
    group_count = jnp.dot(earlier, ones_where(in_group), preferred_element_type=F32)
    group_rank = jnp.sum(jnp.where(in_group, group_count, 0.0), axis=1, keepdims=True)
    base = group * per_group
    facts = [
        (first.astype(F32) - base) * cap + rank0 + 1.0,
        (second.astype(F32) - base) * cap + rank1 + 1.0,
        route_weight[:, 0:1],
        route_weight[:, 1:2],
    ]
    slot = group * slots + group_rank
    by_lane = jnp.broadcast_to(slot, (tokens, tokens)).T
    slot_row = lax.broadcasted_iota(jnp.int32, (slots, tokens), 0).astype(F32)
    token_hot[...] = ones_where(
        slot == lax.broadcasted_iota(jnp.int32, (tokens, GROUPS * slots), 1).astype(F32)
    )
    for g in range(GROUPS):
        slot_hot[g] = ones_where(by_lane[:slots] - float(g * slots) == slot_row)
        hot = (slot - float(g * slots) == lane) & (col < slots)
        rows = [jnp.sum(jnp.where(hot, f, 0.0), axis=0, keepdims=True) for f in facts]
        rows = [rows[0] - 1.0, rows[1] - 1.0, rows[2], rows[3]]
        meta[g] = jnp.concatenate(rows + [jnp.zeros((4, tokens), F32)], axis=0)
    tables[plane] = meta[plane]

    wide_source = lax.broadcasted_iota(jnp.int32, (2 * tokens, 2 * tokens), 0)
    wide_col = lax.broadcasted_iota(jnp.int32, (2 * tokens, 2 * tokens), 1)
    source = jnp.where(wide_source >= tokens, wide_source - tokens, wide_source)
    summer = jnp.where((wide_col >= tokens) | (source > wide_col), -1.0, 0.0).astype(BF16)
    pair = 2 if n_sp % 2 == 0 else 1
    span = pair * tokens
    tile_row = lax.broadcasted_iota(jnp.int32, (span, tokens), 0)
    tile_col = lax.broadcasted_iota(jnp.int32, (span, tokens), 1)
    scale = LOG2E / math.sqrt(HD)

    def attend(h, i):
        q = q_all[h, i * span : (i + 1) * span]
        carry = jnp.zeros((span, tokens), F32)
        total = jnp.zeros((span, HD), F32)
        for j in range(i, -1, -1):
            k = k_all[h, j * span : (j + 1) * span]
            z_pair = lax.dot_general(q, k, (((1,), (1,)), ((), ())), preferred_element_type=F32)
            parts = [None] * pair
            for b in range(pair - 1, -1, -1):
                z = z_pair[:, b * tokens : (b + 1) * tokens] * scale
                z = z + shift_in[j * pair + b, h : h + 1, :]
                soft = jnp.maximum(z, 0.0) + jnp.log2(1.0 + jnp.exp2(-jnp.abs(z)))
                own = z - soft
                if i == j:
                    causal = tile_col + b * tokens < tile_row
                    soft = jnp.where(causal, soft, 0.0)
                high = soft.astype(BF16)
                low = (soft - high.astype(F32)).astype(BF16)
                sums = jnp.dot(
                    jnp.concatenate([high, low], axis=1), summer, preferred_element_type=F32
                )
                weight = jnp.exp2(own + (sums[:, :tokens] + carry))
                if i == j:
                    weight = jnp.where(causal, weight, 0.0)
                carry = carry + sums[:, tokens:]
                parts[b] = weight.astype(BF16)
            total = total + jnp.dot(
                jnp.concatenate(parts, axis=1) if pair > 1 else parts[0],
                v_all[h, j * span : (j + 1) * span],
                preferred_element_type=F32,
            )
        for b in range(pair):
            t = i * pair + b
            block = total[b * tokens : (b + 1) * tokens]
            att_out[h, t] = jnp.concatenate([block[:half], block[half:]], axis=1).astype(BF16)
        for b in range(pair):
            t = i * pair + b

            @pl.when(me != t)
            def _(t=t):
                remote(
                    att_out.at[h, t], att_in.at[h, me], a_send.at[h], a_recv.at[h], (t, dp)
                )

            @pl.when(me == t)
            def _(t=t):
                att_in[h, t] = att_out[h, t]

    settle(shift_in.at[pl.ds(0, n_sp - 1)], s_recv.at[0])
    for h in range(heads):
        settle(inbox.at[h, pl.ds(0, n_sp - 1)], q_recv.at[h])
        for j in range(n_sp):
            here = slice(j * tokens, (j + 1) * tokens)
            q_all[h, here] = inbox[h, j, :tokens, :HD]
            k_all[h, here] = inbox[h, j, :tokens, HD:]
            v_all[h, j * tokens : j * tokens + half] = inbox[h, j, tokens:, :HD]
            v_all[h, j * tokens + half : (j + 1) * tokens] = inbox[h, j, tokens:, HD:]
        for i in range(n_sp // pair - 1, -1, -1):
            attend(h, i)

    for h in range(heads):
        settle(att_in.at[h, pl.ds(0, n_sp - 1)], a_recv.at[h])
        for p in range(n_sp):
            g = p * heads + h
            block = att_in[h, p]
            att[:half, g * HD : (g + 1) * HD] = block[:, :HD]
            att[half:, g * HD : (g + 1) * HD] = block[:, HD:]
    wide_att = att[...].astype(F32)
    ratio = lax.rsqrt(jnp.mean(wide_att * wide_att, axis=1, keepdims=True) + norm_eps)
    normed = (wide_att * ratio * mix_gain[...]).astype(BF16)
    weight_loads[0].wait()
    weight_loads[1].wait()
    square = jnp.zeros((tokens, 1), F32)
    for cols in chunks:
        block = stream[:, cols].astype(F32) + jnp.dot(
            normed, out_w[:, cols], preferred_element_type=F32
        )
        summed[:, cols] = block
        square = square + jnp.sum(block * block, axis=1, keepdims=True)
    ratio = lax.rsqrt(square / width + norm_eps)
    for cols in chunks:
        hidden[:, cols] = (summed[:, cols] * ratio * post_gain[:, cols]).astype(BF16)

    def put_rows(ref, source, cols, rows):
        if cap % 16 == 0:
            ref[source, :, :, cols] = rows.astype(BF16).reshape(per_group, cap, chunk)
        else:
            for m in range(per_group):
                ref[source, m, :, cols] = rows[m * cap : (m + 1) * cap].astype(BF16)

    def take_rows(ref, source, cols):
        if cap % 16 == 0:
            rows = ref[source, :, :, cols]
            return rows.reshape(lanes, rows.shape[-1])
        return jnp.concatenate(
            [ref[source, m, :, cols].astype(F32) for m in range(per_group)], axis=0
        ).astype(BF16)

    z_copies = {}

    def send_plane(k, c):
        q = others[k]
        packed[q, :, chunks[c]] = jnp.dot(
            slot_hot[q], hidden[:, chunks[c]], preferred_element_type=F32
        ).astype(BF16)
        z_copies[k, c] = remote(
            packed.at[q, :, chunks[c]],
            landed.at[plane, :, chunks[c]],
            z_send.at[k, c],
            z_recv.at[k, c],
            at(q, member),
        )

    pieces = range(len(chunks))
    for k in range(1, GROUPS):
        z_copies[k, -1] = remote(
            meta.at[others[k]],
            tables.at[plane],
            t_send.at[k],
            t_recv.at[k],
            at(others[k], member),
        )
    for c in pieces:
        send_plane(3, c)
        send_plane(1, c)
    for c in pieces:
        send_plane(2, c)
    for cols in chunks:
        landed[plane, :, cols] = jnp.dot(
            slot_hot[plane], hidden[:, cols], preferred_element_type=F32
        ).astype(BF16)

    def fan_out(source, src, dst, cols, send, recv):
        for e in range(1, per_group):
            other = lax.rem(member + e, per_group)
            remote(
                src.at[source, other, :, cols],
                dst.at[source, member, :, cols],
                send,
                recv,
                at(plane, other),
            )
        dst[source, member, :, cols] = src[source, member, :, cols]

    def group_wait(source, ref, cols, sem):
        settle(ref.at[source, pl.ds(0, per_group - 1), :, cols], sem)

    hots = {}

    def deliver(k, c):
        source = others[k]
        if k not in hots:
            if k:
                z_copies[k, -1].wait_recv()
            info = tables[source]
            hots[k] = ones_where(one_hot_rows(info, 0) | one_hot_rows(info, 1))[:, :slots]
        if k:
            z_copies[k, c].wait_recv()
        rows = jnp.dot(hots[k], landed[source, :, chunks[c]], preferred_element_type=F32)
        put_rows(stage, source, chunks[c], rows)
        fan_out(source, stage, got, chunks[c], p_send.at[k, c], p_recv.at[k, c])

    loaded = []

    def experts(k, send):
        source = others[k]
        for c, cols in enumerate(chunks):
            group_wait(source, got, cols, p_recv.at[k, c])
        if not loaded:
            loaded.append(True)
            for load in weight_loads[2:]:
                load.wait()
        rows = take_rows(got, source, slice(None))
        part = min(256, ffn)
        for n in range(0, ffn, part):
            gate = jnp.dot(rows, gate_w[:, n : n + part], preferred_element_type=F32)
            upper = jnp.dot(rows, up_w[:, n : n + part], preferred_element_type=F32)
            inner[:, n : n + part] = (gate / (1.0 + jnp.exp(-gate)) * upper).astype(BF16)
        for c, cols in enumerate(chunks):
            out = jnp.dot(inner[...], down_w[:, cols], preferred_element_type=F32)
            put_rows(reply, source, cols, out)
            if send:
                answer(k, c)

    def answer(k, c):
        fan_out(others[k], reply, back, chunks[c], r_send.at[k, c], r_recv.at[k, c])

    y_copies = {}

    def combine(k):
        source = others[k]
        info = tables[source]
        spread = jnp.where(one_hot_rows(info, 0), info[2:3, :], 0.0) + jnp.where(
            one_hot_rows(info, 1), info[3:4, :], 0.0
        )
        spread = spread.T[:slots]
        high = spread.astype(BF16)
        low = (spread - high.astype(F32)).astype(BF16)
        for c, cols in enumerate(chunks):
            group_wait(source, back, cols, r_recv.at[k, c])
            rows = take_rows(back, source, cols)
            total = jnp.dot(high, rows, preferred_element_type=F32) + jnp.dot(
                low, rows, preferred_element_type=F32
            )
            if k:
                partial[source, :, cols] = total.astype(BF16)
                y_copies[k, c] = remote(
                    partial.at[source, :, cols],
                    returned.at[plane, :, cols],
                    y_send.at[k, c],
                    y_recv.at[k, c],
                    at(source, member),
                )
            else:
                returned[source, :, cols] = total.astype(BF16)

    for c in pieces:
        deliver(0, c)
    for c in pieces:
        deliver(1, c)
        deliver(3, c)
    experts(0, False)
    experts(3, True)
    split = len(chunks) // 2
    for c in pieces[:split]:
        deliver(2, c)
    experts(1, True)
    for c in pieces[split:]:
        deliver(2, c)
    combine(3)
    experts(2, True)
    for c in pieces:
        answer(0, c)
    combine(1)
    combine(2)
    combine(0)

    for c, cols in enumerate(chunks):
        for k in range(1, GROUPS):
            y_copies[k, c].wait_recv()
        rows = returned[:, :, cols].reshape(GROUPS * slots, chunk)
        total = jnp.dot(token_hot[...], rows, preferred_element_type=F32)
        result[:, cols] = (hidden[:, cols].astype(F32) + total).astype(BF16)

    settle(shift_out.at[pl.ds(0, n_sp - 1)], s_send.at[0])
    for h in range(heads):
        settle(outbox.at[h, pl.ds(0, n_sp - 1)], q_send.at[h])
        settle(att_out.at[h, pl.ds(0, n_sp - 1)], a_send.at[h])
    for k in range(GROUPS):
        for c, cols in enumerate(chunks):
            if k:
                z_copies[k, c].wait_send()
                y_copies[k, c].wait_send()
            group_wait(others[k], stage, cols, p_send.at[k, c])
            group_wait(others[k], reply, cols, r_send.at[k, c])
        if k:
            z_copies[k, -1].wait_send()


def on_device(
    n_sp,
    n_dp,
    stream,
    queries,
    keys_in,
    values_in,
    key_shift,
    head_shift,
    mix_gain,
    out_weight,
    post_gain,
    route,
    route_weight,
    w_gate,
    w_up,
    w_down,
):
    tokens, width = stream.shape[1:]
    n_heads = key_shift.shape[2]
    heads = n_heads // n_sp
    mixer = queries.shape[2]
    ffn = w_gate.shape[2]
    per_group = n_sp * n_dp // GROUPS
    cap = tokens // per_group
    slots = tokens // 2
    chunks = width // min(512, width)
    dma = pltpu.SemaphoreType.DMA
    own = pltpu.VMEM((tokens, mixer), BF16)
    box = pltpu.VMEM((heads, n_sp, tokens + tokens // 2, 2 * HD), BF16)
    shifts = pltpu.VMEM((n_sp, 8, tokens), F32)
    line = pltpu.VMEM((heads, n_sp * tokens, HD), BF16)
    att_box = pltpu.VMEM((heads, n_sp, tokens // 2, 2 * HD), BF16)
    table = pltpu.VMEM((GROUPS, 8, tokens), F32)
    wide = pltpu.VMEM((GROUPS, per_group, cap, width), BF16)
    narrow = pltpu.VMEM((GROUPS, slots, width), BF16)
    here = pl.BlockSpec(memory_space=pltpu.VMEM)
    there = pl.BlockSpec(memory_space=pl.ANY)
    out = pl.pallas_call(
        functools.partial(layer_kernel, n_sp, n_dp),
        out_shape=jax.ShapeDtypeStruct((tokens, width), BF16),
        in_specs=[there] * 3 + [here] * 3 + [there, here, there, here, here] + [there] * 3,
        out_specs=here,
        scratch_shapes=[
            own,
            own,
            own,
            box,
            box,
            pltpu.VMEM((tokens, tokens), F32),
            shifts,
            shifts,
            line,
            line,
            line,
            att_box,
            att_box,
            own,
            pltpu.VMEM((tokens, width), BF16),
            pltpu.VMEM((tokens, width), F32),
            pltpu.VMEM((tokens, width), BF16),
            table,
            pltpu.VMEM((GROUPS, slots, tokens), BF16),
            pltpu.VMEM((tokens, GROUPS * slots), BF16),
            narrow,
            narrow,
            table,
            wide,
            wide,
            pltpu.VMEM((per_group * cap, ffn), BF16),
            wide,
            wide,
            narrow,
            narrow,
            pltpu.VMEM((mixer, width), BF16),
            pltpu.VMEM((width, ffn), BF16),
            pltpu.VMEM((width, ffn), BF16),
            pltpu.VMEM((ffn, width), BF16),
            dma((3,)),
            dma((5,)),
            dma((1,)),
            dma((1,)),
            dma((heads,)),
            dma((heads,)),
            dma((heads,)),
            dma((heads,)),
            dma((GROUPS,)),
            dma((GROUPS,)),
        ]
        + [dma((GROUPS, chunks))] * 8,
        compiler_params=pltpu.CompilerParams(
            collective_id=0, has_side_effects=True, vmem_limit_bytes=VLIM
        ),
        name="layer",
    )(
        queries[0],
        keys_in[0],
        values_in[0],
        key_shift[0],
        head_shift[None],
        mix_gain[None],
        out_weight,
        post_gain[None],
        stream[0],
        route[0],
        route_weight[0],
        w_gate[0],
        w_up[0],
        w_down[0],
    )
    return out[None]


def solution(mesh):
    return jax.shard_map(
        functools.partial(on_device, mesh.shape["sp"], mesh.shape["dp"]),
        mesh=mesh,
        in_specs=(
            P("dp", "sp", None),
            P("dp", "sp", None),
            P("dp", "sp", None),
            P("dp", "sp", None),
            P("dp", "sp", None),
            P(),
            P(),
            P(),
            P(),
            P("dp", "sp", None),
            P("dp", "sp", None),
            P(("sp", "dp"), None, None),
            P(("sp", "dp"), None, None),
            P(("sp", "dp"), None, None),
        ),
        out_specs=P("dp", "sp", None),
        check_vma=False,
    )
```

time: 137 us -> 107 us (0.78)
  the two profiles are of different devices: /device:TPU:13 before, /device:TPU:0 now
where the time goes in v2:
time: 107 us
  Pallas kernels  100 us (93%)
  local copies, waits for them, and re-layouts  6.09 us (6%)
    pallas_call x1, Pallas kernels, on_device(): pl.pallas_call(functools.partial(layer_kernel, n_sp, n_dp), out_shape=jax...  100 us
    unnamed x4, local copies, waits for them, and re-layouts  6.09 us

profile of v2, /device:TPU:0, one launch (start us, length us, event | category | flops | bytes accessed | tf_op | source)
XLA Modules:
  0.0 106.6 jit_solution(5411010383118820724)
XLA Ops:
  0.0 1.4 %copy.15 = bf16[1,128,16]{2,1,0:T(8,128)(2,1)} copy(bf16[1,128,16]{1,2,0:T(8,128)(2,1)} %param.18) | data formatting | bytes 8192 | tf_op args[4]
  1.4 1.4 %copy.16 = s32[1,128,2]{2,1,0:T(8,128)} copy(s32[1,128,2]{1,2,0:T(2,128)} %param.23) | data formatting | bytes 2048 | tf_op args[9]
  2.8 1.4 %copy.17 = f32[1,128,2]{2,1,0:T(8,128)} copy(f32[1,128,2]{1,2,0:T(2,128)} %param.24) | data formatting | bytes 2048 | tf_op args[10]
  4.2 100.5 %layer.1 = bf16[128,2048]{1,0:T(8,128)(2,1)} custom-call(bf16[128,1024]{1,0:T(8,128)(2,1)} %bitcast.19, bf16[128,1024]{1,0:T(8,128)(2,1)} %bitcast.20, bf16[128,1024]{1,0:T(8,128)(2,1)} %bitcast.21, bf16[128,16]{1,0:T(8,128)(2,1)} %bitcast.24, f32[1,16]{1,0:T(1,128)} %bitcast.27, f32[1,1024]{1,0:T(1,128)} %bitcast.26, bf16[1024,2048]{1,0:T(8,128)(2,1)} %out_hbm.1, ...), custom_call_target="tpu_custom_call" | custom-call | tf_op jit(solution)/shard_map/layer/pallas_call | solution.py:555
  104.7 1.9 %copy.19 = bf16[1,128,2048]{2,1,0:T(8,128)(2,1)} copy(bf16[1,128,2048]{2,1,0:T(8,128)(2,1)} %bitcast.17) | data formatting | bytes 1048576

commit v3 on v2

--- a/solution.py
+++ b/solution.py
@@ -34,24 +34,29 @@
     queries,
     keys_in,
     values_in,
-    key_shift,
-    head_shift,
-    mix_gain,
+    key_shift_hbm,
+    head_shift_hbm,
+    mix_gain_hbm,
     out_hbm,
-    post_gain,
+    post_gain_hbm,
     stream_hbm,
-    route,
-    route_weight,
+    route_hbm,
+    route_weight_hbm,
     gate_hbm,
     up_hbm,
     down_hbm,
     result,
+    key_shift,
+    head_shift,
+    mix_gain,
+    post_gain,
+    route,
+    route_weight,
     q_own,
     k_own,
     v_own,
     outbox,
     inbox,
-    shift_pad,
     shift_out,
     shift_in,
     q_all,
@@ -81,6 +86,7 @@
     up_w,
     down_w,
     i_sem,
+    n_sem,
     w_sem,
     s_send,
     s_recv,
@@ -138,7 +144,20 @@
         pltpu.make_async_copy(keys_in, k_own, i_sem.at[1]),
         pltpu.make_async_copy(values_in, v_own, i_sem.at[2]),
     ]
-    for load in qkv_loads:
+    small_loads = [
+        pltpu.make_async_copy(src, dst, n_sem.at[i])
+        for i, (src, dst) in enumerate(
+            (
+                (key_shift_hbm, key_shift),
+                (head_shift_hbm, head_shift),
+                (route_hbm, route),
+                (route_weight_hbm, route_weight),
+                (mix_gain_hbm, mix_gain),
+                (post_gain_hbm, post_gain),
+            )
+        )
+    ]
+    for load in qkv_loads + small_loads:
         load.start()
     barrier = pltpu.get_barrier_semaphore()
     for d in range(1, n_sp):
@@ -154,10 +173,15 @@
                 device_id_type=MESH,
             )
 
-    n_heads = key_shift.shape[1]
-    shift_pad[...] = jnp.zeros_like(shift_pad)
-    shift_pad[:, :n_heads] = (key_shift[...].astype(F32) + head_shift[...]) * LOG2E
-    turned = shift_pad[...].T
+    for load in small_loads[:2]:
+        load.wait()
+
+    n_heads = key_shift.shape[0]
+    same = lax.broadcasted_iota(jnp.int32, (n_heads, n_heads), 0) == lax.broadcasted_iota(
+        jnp.int32, (n_heads, n_heads), 1
+    )
+    head_column = jnp.sum(jnp.where(same, head_shift[...], 0.0), axis=1, keepdims=True)
+    turned = (key_shift[...].astype(F32) + head_column) * LOG2E
     for p in range(n_sp):
         shift_out[p, :heads, :] = turned[p * heads : (p + 1) * heads]
     shift_in[me] = shift_out[me]
@@ -201,15 +225,21 @@
     send_head(0)
     for h in range(1, heads):
         pack_head(h)
-        send_head(h)
+
+    for load in small_loads[2:]:
+        load.wait()
 
     row = lax.broadcasted_iota(jnp.int32, (tokens, tokens), 0)
     col = lax.broadcasted_iota(jnp.int32, (tokens, tokens), 1)
     earlier = ones_where(row > col)
     n_expert = n_sp * n_dp
     wide = max(tokens, n_expert)
-    expert = lax.broadcasted_iota(jnp.int32, (tokens, wide), 1)
-    first, second = route[:, 0:1], route[:, 1:2]
+    expert = lax.broadcasted_iota(jnp.int32, (tokens, wide), 1).astype(F32)
+
+    def column(values):
+        return jnp.sum(jnp.where(row == col, values, 0.0), axis=1, keepdims=True)
+
+    first, second = (column(route[k : k + 1, :].astype(F32)) for k in range(2))
     hit0, hit1 = first == expert, second == expert
     count0 = jnp.dot(earlier, ones_where(hit0), preferred_element_type=F32)
     count1 = jnp.dot(earlier, ones_where(hit1), preferred_element_type=F32) + jnp.dot(
@@ -219,17 +249,17 @@
     rank1 = jnp.sum(jnp.where(hit1, count1, 0.0), axis=1, keepdims=True)
     group = jnp.zeros((tokens, 1), F32)
     for g in range(1, GROUPS):
-        group = group + jnp.where(first >= g * per_group, 1.0, 0.0)
+        group = group + jnp.where(first >= float(g * per_group), 1.0, 0.0)
     lane = col.astype(F32)
     in_group = lane == group
     group_count = jnp.dot(earlier, ones_where(in_group), preferred_element_type=F32)
     group_rank = jnp.sum(jnp.where(in_group, group_count, 0.0), axis=1, keepdims=True)
     base = group * per_group
     facts = [
-        (first.astype(F32) - base) * cap + rank0 + 1.0,
-        (second.astype(F32) - base) * cap + rank1 + 1.0,
-        route_weight[:, 0:1],
-        route_weight[:, 1:2],
+        (first - base) * cap + rank0 + 1.0,
+        (second - base) * cap + rank1 + 1.0,
+        column(route_weight[0:1, :]),
+        column(route_weight[1:2, :]),
     ]
     slot = group * slots + group_rank
     by_lane = jnp.broadcast_to(slot, (tokens, tokens)).T
@@ -248,7 +278,7 @@
     wide_source = lax.broadcasted_iota(jnp.int32, (2 * tokens, 2 * tokens), 0)
     wide_col = lax.broadcasted_iota(jnp.int32, (2 * tokens, 2 * tokens), 1)
     source = jnp.where(wide_source >= tokens, wide_source - tokens, wide_source)
-    summer = jnp.where((wide_col >= tokens) | (source > wide_col), -1.0, 0.0).astype(BF16)
+    summer = jnp.where((wide_col >= tokens) | (source >= wide_col), -1.0, 0.0).astype(BF16)
     pair = 2 if n_sp % 2 == 0 else 1
     span = pair * tokens
     tile_row = lax.broadcasted_iota(jnp.int32, (span, tokens), 0)
@@ -266,8 +296,7 @@
             for b in range(pair - 1, -1, -1):
                 z = z_pair[:, b * tokens : (b + 1) * tokens] * scale
                 z = z + shift_in[j * pair + b, h : h + 1, :]
-                soft = jnp.maximum(z, 0.0) + jnp.log2(1.0 + jnp.exp2(-jnp.abs(z)))
-                own = z - soft
+                soft = jnp.maximum(z, jnp.log2(1.0 + jnp.exp2(jnp.minimum(z, 100.0))))
                 if i == j:
                     causal = tile_col + b * tokens < tile_row
                     soft = jnp.where(causal, soft, 0.0)
@@ -276,7 +305,7 @@
                 sums = jnp.dot(
                     jnp.concatenate([high, low], axis=1), summer, preferred_element_type=F32
                 )
-                weight = jnp.exp2(own + (sums[:, :tokens] + carry))
+                weight = jnp.exp2(z + (sums[:, :tokens] + carry))
                 if i == j:
                     weight = jnp.where(causal, weight, 0.0)
                 carry = carry + sums[:, tokens:]
@@ -290,6 +319,7 @@
             t = i * pair + b
             block = total[b * tokens : (b + 1) * tokens]
             att_out[h, t] = jnp.concatenate([block[:half], block[half:]], axis=1).astype(BF16)
+    def return_head(h, i):
         for b in range(pair):
             t = i * pair + b
 
@@ -305,7 +335,13 @@
 
     settle(shift_in.at[pl.ds(0, n_sp - 1)], s_recv.at[0])
     for h in range(heads):
+        settle(outbox.at[h, pl.ds(0, n_sp - 1)], q_send.at[h])
+        if h + 1 < heads:
+            send_head(h + 1)
         settle(inbox.at[h, pl.ds(0, n_sp - 1)], q_recv.at[h])
+        if h:
+            for i in range(n_sp // pair - 1, -1, -1):
+                return_head(h - 1, i)
         for j in range(n_sp):
             here = slice(j * tokens, (j + 1) * tokens)
             q_all[h, here] = inbox[h, j, :tokens, :HD]
@@ -314,6 +350,8 @@
             v_all[h, j * tokens + half : (j + 1) * tokens] = inbox[h, j, tokens:, HD:]
         for i in range(n_sp // pair - 1, -1, -1):
             attend(h, i)
+            if h + 1 == heads:
+                return_head(h, i)
 
     for h in range(heads):
         settle(att_in.at[h, pl.ds(0, n_sp - 1)], a_recv.at[h])
@@ -380,8 +418,6 @@
     for c in pieces:
         send_plane(3, c)
         send_plane(1, c)
-    for c in pieces:
-        send_plane(2, c)
     for cols in chunks:
         landed[plane, :, cols] = jnp.dot(
             slot_hot[plane], hidden[:, cols], preferred_element_type=F32
@@ -444,53 +480,62 @@
 
     y_copies = {}
 
-    def combine(k):
+    spreads = {}
+
+    def combine(k, c):
         source = others[k]
-        info = tables[source]
-        spread = jnp.where(one_hot_rows(info, 0), info[2:3, :], 0.0) + jnp.where(
-            one_hot_rows(info, 1), info[3:4, :], 0.0
+        cols = chunks[c]
+        if k not in spreads:
+            info = tables[source]
+            spread = jnp.where(one_hot_rows(info, 0), info[2:3, :], 0.0) + jnp.where(
+                one_hot_rows(info, 1), info[3:4, :], 0.0
+            )
+            spread = spread.T[:slots]
+            high = spread.astype(BF16)
+            spreads[k] = high, (spread - high.astype(F32)).astype(BF16)
+        high, low = spreads[k]
+        group_wait(source, back, cols, r_recv.at[k, c])
+        rows = take_rows(back, source, cols)
+        total = jnp.dot(high, rows, preferred_element_type=F32) + jnp.dot(
+            low, rows, preferred_element_type=F32
         )
-        spread = spread.T[:slots]
-        high = spread.astype(BF16)
-        low = (spread - high.astype(F32)).astype(BF16)
-        for c, cols in enumerate(chunks):
-            group_wait(source, back, cols, r_recv.at[k, c])
-            rows = take_rows(back, source, cols)
-            total = jnp.dot(high, rows, preferred_element_type=F32) + jnp.dot(
-                low, rows, preferred_element_type=F32
+        if k:
+            partial[source, :, cols] = total.astype(BF16)
+            y_copies[k, c] = remote(
+                partial.at[source, :, cols],
+                returned.at[plane, :, cols],
+                y_send.at[k, c],
+                y_recv.at[k, c],
+                at(source, member),
             )
-            if k:
-                partial[source, :, cols] = total.astype(BF16)
-                y_copies[k, c] = remote(
-                    partial.at[source, :, cols],
-                    returned.at[plane, :, cols],
-                    y_send.at[k, c],
-                    y_recv.at[k, c],
-                    at(source, member),
-                )
-            else:
-                returned[source, :, cols] = total.astype(BF16)
+        else:
+            returned[source, :, cols] = total.astype(BF16)
 
     for c in pieces:
         deliver(0, c)
     for c in pieces:
         deliver(1, c)
         deliver(3, c)
+        send_plane(2, c)
     experts(0, False)
-    experts(3, True)
-    split = len(chunks) // 2
-    for c in pieces[:split]:
+    experts(3, False)
+    experts(1, False)
+    for c in pieces:
         deliver(2, c)
-    experts(1, True)
-    for c in pieces[split:]:
-        deliver(2, c)
-    combine(3)
-    experts(2, True)
-    for c in pieces:
+    for c in pieces:
+        answer(3, c)
+    experts(2, False)
+    for c in pieces:
+        combine(3, c)
+        answer(2, c)
+    for c in pieces:
+        combine(2, c)
+        answer(1, c)
+    for c in pieces:
+        combine(1, c)
         answer(0, c)
-    combine(1)
-    combine(2)
-    combine(0)
+    for c in pieces:
+        combine(0, c)
 
     for c, cols in enumerate(chunks):
         for k in range(1, GROUPS):
@@ -501,7 +546,6 @@
 
     settle(shift_out.at[pl.ds(0, n_sp - 1)], s_send.at[0])
     for h in range(heads):
-        settle(outbox.at[h, pl.ds(0, n_sp - 1)], q_send.at[h])
         settle(att_out.at[h, pl.ds(0, n_sp - 1)], a_send.at[h])
     for k in range(GROUPS):
         for c, cols in enumerate(chunks):
@@ -554,16 +598,21 @@
     there = pl.BlockSpec(memory_space=pl.ANY)
     out = pl.pallas_call(
         functools.partial(layer_kernel, n_sp, n_dp),
-        out_shape=jax.ShapeDtypeStruct((tokens, width), BF16),
-        in_specs=[there] * 3 + [here] * 3 + [there, here, there, here, here] + [there] * 3,
+        out_shape=pltpu.VMEM((tokens, width), BF16),
+        in_specs=[there] * 14,
         out_specs=here,
         scratch_shapes=[
+            pltpu.VMEM((n_heads, tokens), BF16),
+            pltpu.VMEM((1, n_heads), F32),
+            pltpu.VMEM((1, mixer), F32),
+            pltpu.VMEM((1, width), F32),
+            pltpu.VMEM((2, tokens), jnp.int32),
+            pltpu.VMEM((2, tokens), F32),
             own,
             own,
             own,
             box,
             box,
-            pltpu.VMEM((tokens, tokens), F32),
             shifts,
             shifts,
             line,
@@ -593,6 +642,7 @@
             pltpu.VMEM((width, ffn), BF16),
             pltpu.VMEM((ffn, width), BF16),
             dma((3,)),
+            dma((6,)),
             dma((5,)),
             dma((1,)),
             dma((1,)),
@@ -612,14 +662,14 @@
         queries[0],
         keys_in[0],
         values_in[0],
-        key_shift[0],
+        key_shift[0].T,
         head_shift[None],
         mix_gain[None],
         out_weight,
         post_gain[None],
         stream[0],
-        route[0],
-        route_weight[0],
+        route[0].T,
+        route_weight[0].T,
         w_gate[0],
         w_up[0],
         w_down[0],

time: 107 us -> 94.9 us (0.89)
  Pallas kernels: 100 us -> 94 us
  local copies, waits for them, and re-layouts: 6.09 us -> 0.8 us
    pallas_call x1, Pallas kernels: 100 us -> 94 us  [on_device(): pl.pallas_call(functools.partial(layer_kernel, n_sp, n_dp), out_shape=plt...]
    unnamed x4 -> x1, local copies, waits for them, and re-layouts: 6.09 us -> 0.8 us
where the time goes in v3:
time: 94.9 us; the launch traced here: 94.8 us
  Pallas kernels  94 us (99%)
    pallas_call x1, Pallas kernels, on_device(): pl.pallas_call(functools.partial(layer_kernel, n_sp, n_dp), out_shape=plt...  94 us

profile of v3, /device:TPU:0, one launch (start us, length us, event | category | flops | bytes accessed | tf_op | source)
XLA Modules:
  0.0 94.8 jit_solution(9904127334077489507)
XLA Ops:
  0.0 94.0 %layer.1 = bf16[128,2048]{1,0:T(8,128)(2,1)S(1)} custom-call(bf16[128,1024]{1,0:T(8,128)(2,1)} %bitcast.25, bf16[128,1024]{1,0:T(8,128)(2,1)} %bitcast.26, bf16[128,1024]{1,0:T(8,128)(2,1)} %bitcast.27, bf16[16,128]{1,0:T(8,128)(2,1)} %bitcast.29, f32[1,16]{1,0:T(1,128)} %bitcast.33, f32[1,1024]{1,0:T(1,128)} %bitcast.30, bf16[1024,2048]{1,0:T(8,128)(2,1)} %out_hbm.1, ...), custom_call_target="tpu_custom_call" | custom-call | tf_op jit(solution)/shard_map/layer/pallas_call | solution.py:599
  94.0 0.8 copy.16
